TPU v7x, 32 devices: a whole 2x2x4 slice. The times are simulated.
32 devices in a mesh: fs: 8 (over z, y), tp: 4 (over x, core).
Axes of the slice: x: 2, y: 2, z: 4, core: 2. Of those that a mesh axis runs over, the one named last changes fastest.
Arguments:
- saved_input: bfloat16 [16384, 2048], P('fs'), may hold values from -6 to 6
- query_cotangent: bfloat16 [16384, 2048], P('fs', 'tp'), may hold values from -0.046875 to 0.046875
- forget_cotangent: bfloat16 [16384, 2048], P('fs', 'tp'), may hold values from -0.046875 to 0.046875
- mixed_output: bfloat16 [16384, 2048], P('fs', 'tp'), may hold values from -6 to 6
- out_cotangent: bfloat16 [16384, 2048], P('fs'), may hold values from -0.046875 to 0.046875
- query_basis: bfloat16 [2048, 256], replicated, may hold values from -0.125 to 0.125
- forget_basis: bfloat16 [2048, 256], replicated, may hold values from -0.125 to 0.125
- out_basis: bfloat16 [2048, 256], replicated, may hold values from -0.125 to 0.125
- query_weight: float32 [2048, 2048], P('fs', 'tp'), may hold values from -0.125 to 0.125
- forget_weight: float32 [2048, 2048], P('fs', 'tp'), may hold values from -0.125 to 0.125
- out_weight: float32 [2048, 2048], P('fs', 'tp'), may hold values from -0.125 to 0.125
- query_first: float32 [256, 2048], P('fs', 'tp'), may hold values from -25 to 25
- forget_first: float32 [256, 2048], P('fs', 'tp'), may hold values from -25 to 25
- out_first: float32 [256, 2048], P('fs', 'tp'), may hold values from -25 to 25
- query_second: float32 [256, 2048], P('fs', 'tp'), may hold values from 0.2 to 2
- forget_second: float32 [256, 2048], P('fs', 'tp'), may hold values from 0.2 to 2
- out_second: float32 [256, 2048], P('fs', 'tp'), may hold values from 0.2 to 2
Outputs:
- query_update: float32 [2048, 2048], P('fs', 'tp')
- forget_update: float32 [2048, 2048], P('fs', 'tp')
- out_update: float32 [2048, 2048], P('fs', 'tp')
- query_first_new: float32 [256, 2048], P('fs', 'tp')
- forget_first_new: float32 [256, 2048], P('fs', 'tp')
- out_first_new: float32 [256, 2048], P('fs', 'tp')
- query_second_new: float32 [256, 2048], P('fs', 'tp')
- forget_second_new: float32 [256, 2048], P('fs', 'tp')
- out_second_new: float32 [256, 2048], P('fs', 'tp')
- query_copy: bfloat16 [2048, 2048], P(None, 'tp')
- forget_copy: bfloat16 [2048, 2048], P(None, 'tp')
- out_copy: bfloat16 [2048, 2048], P(None, 'tp')
All inputs are finite; a program needn't handle non-finite values.
Results may differ from a plain program's by a relative error of at most 0.0065.
Values may be sent and summed in bfloat16 or wider, within the bound.
A program may use at most 128 MiB of HBM per device.

v0:
```python
import jax
import jax.numpy as jnp
from jax import lax
from jax.sharding import PartitionSpec as P

WIDTH = 2048
RANK = 256


highest = lax.Precision.HIGHEST


def contract_rows(left, right):
    return lax.dot_general(
        left, right, (((0,), (0,)), ((), ())), precision=None, preferred_element_type=jnp.float32
    )


def moments(source, cotangent, basis, weight, first, second):
    row_count = weight.shape[0]
    basis_rows = lax.dynamic_slice_in_dim(
        basis, lax.axis_index("fs") * row_count, row_count, 0
    ).astype(jnp.float32)
    reduced = jnp.dot(source, basis, preferred_element_type=jnp.float32)
    reduced_high = reduced.astype(jnp.bfloat16)
    reduced_low = (reduced - reduced_high.astype(jnp.float32)).astype(jnp.bfloat16)
    projected = lax.psum_scatter(
        (contract_rows(reduced_high, cotangent) + contract_rows(reduced_low, cotangent)).astype(
            jnp.bfloat16
        ),
        "fs",
        scatter_dimension=0,
        tiled=True,
    ).astype(jnp.float32)
    first_new = 0.8 * first + 0.2 * projected
    second_new = 0.95 * second + 0.05 * projected * projected
    direction = first_new / (jnp.sqrt(second_new) + 1e-08)
    return (direction, first_new, second_new, jnp.sum(direction * direction), basis_rows)


def expand(direction, basis_rows, total, weight):
    stepped = jnp.dot(
        basis_rows, lax.all_gather(direction, "fs", axis=0, tiled=True), precision=highest
    )
    update = stepped * lax.rsqrt(total / (RANK * WIDTH) + 1e-06)
    return (update, (weight - 0.05 * update).astype(jnp.bfloat16))


def local(
    saved_input,
    query_cotangent,
    forget_cotangent,
    mixed_output,
    out_cotangent,
    query_basis,
    forget_basis,
    out_basis,
    query_weight,
    forget_weight,
    out_weight,
    query_first,
    forget_first,
    out_first,
    query_second,
    forget_second,
    out_second,
):
    query_dir, query_one, query_two, query_sq, query_rows = moments(
        saved_input, query_cotangent, query_basis, query_weight, query_first, query_second
    )
    forget_dir, forget_one, forget_two, forget_sq, forget_rows = moments(
        saved_input, forget_cotangent, forget_basis, forget_weight, forget_first, forget_second
    )
    out_dir, out_one, out_two, out_sq, out_rows = moments(
        out_cotangent, mixed_output, out_basis, out_weight, out_first, out_second
    )
    totals = lax.psum((query_sq, forget_sq, out_sq), ("fs", "tp"))
    query_step, query_new = expand(query_dir, query_rows, totals[0], query_weight)
    forget_step, forget_new = expand(forget_dir, forget_rows, totals[1], forget_weight)
    out_step, out_new = expand(out_dir, out_rows, totals[2], out_weight)
    query_copy, forget_copy, out_copy = (
        lax.all_gather(query_new, "fs", axis=0, tiled=True),
        lax.all_gather(forget_new, "fs", axis=0, tiled=True),
        lax.all_gather(out_new, "fs", axis=0, tiled=True),
    )
    return (
        query_step,
        forget_step,
        out_step,
        query_one,
        forget_one,
        out_one,
        query_two,
        forget_two,
        out_two,
        query_copy,
        forget_copy,
        out_copy,
    )


def solution(mesh):
    in_specs = (
        P("fs", None),
        P("fs", "tp"),
        P("fs", "tp"),
        P("fs", "tp"),
        P("fs", None),
        P(),
        P(),
        P(),
        P("fs", "tp"),
        P("fs", "tp"),
        P("fs", "tp"),
        P("fs", "tp"),
        P("fs", "tp"),
        P("fs", "tp"),
        P("fs", "tp"),
        P("fs", "tp"),
        P("fs", "tp"),
    )
    out_specs = (
        P("fs", "tp"),
        P("fs", "tp"),
        P("fs", "tp"),
        P("fs", "tp"),
        P("fs", "tp"),
        P("fs", "tp"),
        P("fs", "tp"),
        P("fs", "tp"),
        P("fs", "tp"),
        P(None, "tp"),
        P(None, "tp"),
        P(None, "tp"),
    )
    return jax.shard_map(local, mesh=mesh, in_specs=in_specs, out_specs=out_specs, check_vma=False)
```

profile of v0, /device:TPU:0, one launch (start us, length us, event | category | flops | bytes accessed | tf_op | source)
XLA Modules:
  0.0 426.3 jit_solution(11486083367784151921)
XLA Ops:
  7.2 6.2 %fusion.31 = f32[2048,256]{1,0:T(8,128)S(1)} fusion(bf16[2048,2048]{1,0:T(8,128)(2,1)} %param.17, bf16[2048,256]{1,0:T(8,128)(2,1)} %param.23), kind=kOutput, calls=%fused_computation.49 | convolution fusion | flops 2147483648 | bytes 11534336 | tf_op jit(solution)/shard_map/dot_general | solution.py:24
  14.3 1.5 fusion.1
  15.9 6.0 %fusion.32 = f32[2048,256]{1,0:T(8,128)S(1)} fusion(bf16[2048,2048]{1,0:T(8,128)(2,1)} %param.21, bf16[2048,256]{1,0:T(8,128)(2,1)S(1)} %copy-done.13), kind=kOutput, calls=%fused_computation.50 | convolution fusion | flops 2147483648 | bytes 11534336 | tf_op jit(solution)/shard_map/dot_general | solution.py:24
  22.6 1.4 fusion.2
  24.2 6.0 %fusion.30 = f32[2048,256]{1,0:T(8,128)S(1)} fusion(bf16[2048,2048]{1,0:T(8,128)(2,1)} %param.17, bf16[2048,256]{1,0:T(8,128)(2,1)S(1)} %copy-done.14), kind=kOutput, calls=%fused_computation.48 | convolution fusion | flops 2147483648 | bytes 11534336 | tf_op jit(solution)/shard_map/dot_general | solution.py:24
  31.1 1.5 fusion
  32.6 48.1 %reduce-scatter.6.cloned.1.call-done = bf16[32,512]{1,0:T(8,128)(2,1)} async-done(((bf16[256,512]{1,0:T(8,128)(2,1)}), bf16[32,512]{1,0:T(8,128)(2,1)}) %reduce-scatter.6.cloned.1.call-update) | async-done | bytes 32784 | tf_op jit(solution)/shard_map/reduce_scatter | solution.py:27
  80.8 2.0 multiply_reduce_fusion.1
  82.8 31.7 %all_gather.19 = f32[256,512]{1,0:T(8,128)S(1)} all-gather(f32[32,512]{1,0:T(8,128)S(1)} %get-tuple-element.20), channel_id=1, replica_groups=mesh['fs'=8,'tp'=4] {'fs'}, dimensions={0}, use_global_device_ids=true | all-gather | bytes 589824 | tf_op jit(solution)/shard_map/all_gather | solution.py:43
  114.5 31.3 %reduce-scatter.8.cloned.1.call-done = bf16[32,512]{1,0:T(8,128)(2,1)} async-done(((bf16[256,512]{1,0:T(8,128)(2,1)}), bf16[32,512]{1,0:T(8,128)(2,1)}) %reduce-scatter.8.cloned.1.call-update) | async-done | bytes 32784 | tf_op jit(solution)/shard_map/reduce_scatter | solution.py:27
  145.8 2.0 multiply_reduce_fusion
  147.9 63.0 %reduce-scatter.4.cloned.1.call-done = bf16[32,512]{1,0:T(8,128)(2,1)} async-done(((bf16[256,512]{1,0:T(8,128)(2,1)}), bf16[32,512]{1,0:T(8,128)(2,1)}) %reduce-scatter.4.cloned.1.call-update) | async-done | bytes 32784 | tf_op jit(solution)/shard_map/reduce_scatter | solution.py:27
  210.9 2.0 multiply_reduce_fusion.2
  212.9 40.4 %all-reduce = (f32[]{:T(128)}, f32[]{:T(128)}, f32[]{:T(128)}) all-reduce(f32[]{:T(128)} %get-tuple-element.23, f32[]{:T(128)} %get-tuple-element.19, f32[]{:T(128)} %get-tuple-element.15), channel_id=1, replica_groups=mesh['fs'=8,'tp'=4] {'fs','tp'}, use_global_device_ids=true, to_apply=%region_2.0 | all-reduce | flops 3 | bytes 24 | tf_op jit(solution)/shard_map/psum | solution.py:77
  254.0 2.3 subtract_convert_fusion.7
  257.1 32.5 %all_gather.20 = f32[256,512]{1,0:T(8,128)S(1)} all-gather(f32[32,512]{1,0:T(8,128)S(1)} %get-tuple-element.16), channel_id=1, replica_groups=mesh['fs'=8,'tp'=4] {'fs'}, dimensions={0}, use_global_device_ids=true | all-gather | bytes 589824 | tf_op jit(solution)/shard_map/all_gather | solution.py:43
  289.6 2.5 subtract_convert_fusion.6
  292.8 32.1 %all_gather.18 = f32[256,512]{1,0:T(8,128)S(1)} all-gather(f32[32,512]{1,0:T(8,128)S(1)} %get-tuple-element.24), channel_id=1, replica_groups=mesh['fs'=8,'tp'=4] {'fs'}, dimensions={0}, use_global_device_ids=true | all-gather | bytes 589824 | tf_op jit(solution)/shard_map/all_gather | solution.py:43
  324.9 2.3 subtract_convert_fusion.8
  327.2 35.1 %all-gather.8.cloned.1.call-done = bf16[2048,512]{1,0:T(8,128)(2,1)} async-done(((bf16[256,512]{1,0:T(8,128)(2,1)}), bf16[2048,512]{1,0:T(8,128)(2,1)}) %all-gather.8.cloned.1.call-update) | async-done | bytes 2097168 | tf_op jit(solution)/shard_map/all_gather | solution.py:84
  362.4 50.2 %all-gather.4.cloned.1.call-done = bf16[2048,512]{1,0:T(8,128)(2,1)} async-done(((bf16[256,512]{1,0:T(8,128)(2,1)}), bf16[2048,512]{1,0:T(8,128)(2,1)}) %all-gather.4.cloned.1.call-update) | async-done | bytes 2097168 | tf_op jit(solution)/shard_map/all_gather | solution.py:82
  412.6 3.2 copy.32
  415.8 1.3 copy.33
  418.1 1.3 copy.34
  (46 shorter events, 3.7 us)
Async XLA Ops:
  7.2 6.3 %copy-start = (bf16[2048,512]{1,0:T(8,128)(2,1)S(1)}, bf16[2048,512]{1,0:T(8,128)(2,1)}, u32[]{:S(2)}) copy-start(bf16[2048,512]{1,0:T(8,128)(2,1)} %param.19) | copy-start | bytes 6291460
  7.2 73.6 %reduce-scatter.6.cloned.1.call-start = ((), (), s32[]{:S(2)}) async-start(), calls=%async_computation.4 | async-start | bytes 294912 | tf_op jit(solution)/shard_map/reduce_scatter | solution.py:27
  14.3 1.6 copy-start.13
  15.8 130.0 %reduce-scatter.8.cloned.1.call-start = ((), (), s32[]{:S(2)}) async-start(), calls=%async_computation.5 | async-start | bytes 294912 | tf_op jit(solution)/shard_map/reduce_scatter | solution.py:27
  15.8 6.0 %copy-start.1 = (bf16[2048,512]{1,0:T(8,128)(2,1)S(1)}, bf16[2048,512]{1,0:T(8,128)(2,1)}, u32[]{:S(2)}) copy-start(bf16[2048,512]{1,0:T(8,128)(2,1)} %param.20) | copy-start | bytes 6291460
  22.6 1.5 copy-start.14
  24.1 186.8 %reduce-scatter.4.cloned.1.call-start = ((), (), s32[]{:S(2)}) async-start(), calls=%async_computation.3 | async-start | bytes 294912 | tf_op jit(solution)/shard_map/reduce_scatter | solution.py:27
  24.2 6.1 %copy-start.2 = (bf16[2048,512]{1,0:T(8,128)(2,1)S(1)}, bf16[2048,512]{1,0:T(8,128)(2,1)}, u32[]{:S(2)}) copy-start(bf16[2048,512]{1,0:T(8,128)(2,1)} %param.18) | copy-start | bytes 6291460
  31.0 49.8 %copy-start.7 = (f32[32,512]{1,0:T(8,128)S(1)}, f32[32,512]{1,0:T(8,128)}, u32[]{:S(2)}) copy-start(f32[32,512]{1,0:T(8,128)} %param.32) | copy-start | bytes 196612
  31.0 49.8 %copy-start.8 = (f32[32,512]{1,0:T(8,128)S(1)}, f32[32,512]{1,0:T(8,128)}, u32[]{:S(2)}) copy-start(f32[32,512]{1,0:T(8,128)} %param.29) | copy-start | bytes 196612
  31.0 114.8 %copy-start.9 = (f32[32,512]{1,0:T(8,128)S(1)}, f32[32,512]{1,0:T(8,128)}, u32[]{:S(2)}) copy-start(f32[32,512]{1,0:T(8,128)} %param.33) | copy-start | bytes 196612
  31.0 114.8 %copy-start.10 = (f32[32,512]{1,0:T(8,128)S(1)}, f32[32,512]{1,0:T(8,128)}, u32[]{:S(2)}) copy-start(f32[32,512]{1,0:T(8,128)} %param.30) | copy-start | bytes 196612
  31.0 179.8 %copy-start.11 = (f32[32,512]{1,0:T(8,128)S(1)}, f32[32,512]{1,0:T(8,128)}, u32[]{:S(2)}) copy-start(f32[32,512]{1,0:T(8,128)} %param.31) | copy-start | bytes 196612
  31.1 179.8 %copy-start.12 = (f32[32,512]{1,0:T(8,128)S(1)}, f32[32,512]{1,0:T(8,128)}, u32[]{:S(2)}) copy-start(f32[32,512]{1,0:T(8,128)} %param.28) | copy-start | bytes 196612
  32.5 221.5 %copy-start.5 = (f32[256,512]{1,0:T(8,128)S(1)}, f32[256,512]{1,0:T(8,128)}, u32[]{:S(2)}) copy-start(f32[256,512]{1,0:T(8,128)} %param.26) | copy-start | bytes 1572868
  32.5 294.7 %all-gather.6.cloned.1.call-start = ((), (), s32[]{:S(2)}) async-start(), calls=%async_computation.7 | async-start | bytes 2359296 | tf_op jit(solution)/shard_map/all_gather | solution.py:83
  256.3 68.7 %copy-start.6 = (f32[256,512]{1,0:T(8,128)S(1)}, f32[256,512]{1,0:T(8,128)}, u32[]{:S(2)}) copy-start(f32[256,512]{1,0:T(8,128)} %param.25) | copy-start | bytes 1572868
  256.3 106.1 %all-gather.8.cloned.1.call-start = ((), (), s32[]{:S(2)}) async-start(), calls=%async_computation.8 | async-start | bytes 2359296 | tf_op jit(solution)/shard_map/all_gather | solution.py:84
  292.1 120.5 %all-gather.4.cloned.1.call-start = ((), (), s32[]{:S(2)}) async-start(), calls=%async_computation.6 | async-start | bytes 2359296 | tf_op jit(solution)/shard_map/all_gather | solution.py:82
  412.6 3.2 copy-start.3
  415.8 2.3 copy-start.4
Sparse Core Ops, SparseCore 0:
  15.9 64.7 reduce-scatter.5
  84.6 61.1 reduce-scatter.7
  149.7 61.1 reduce-scatter.3
  256.4 54.7 all-gather.5
  313.8 48.5 all-gather.7
  364.9 47.6 all-gather.3
where the time goes:
time: 427 us; the launch traced here: 426 us
  waiting for transfers between devices  228 us (53%)
  blocking collectives  137 us (32%)
  matrix products  31.9 us (7%)
  between operations  16.4 us (4%)
  local copies, waits for them, and re-layouts  6.94 us (2%)
  other arithmetic  6.12 us (1%)
    reduce_scatter x3, waiting for transfers between devices, moments(): lax.psum_scatter((contract_rows(reduced_high, cotangent) + contract_rows(...  142 us
    all_gather x3, blocking collectives, expand(): lax.all_gather(direction, 'fs', axis=0, tiled=True)  96.4 us
    all_gather x1, waiting for transfers between devices, local(): lax.all_gather(query_new, 'fs', axis=0, tiled=True)  50.2 us
    psum x1, blocking collectives, local(): totals = lax.psum((query_sq, forget_sq, out_sq), ('fs', 'tp'))  40.4 us
    all_gather x1, waiting for transfers between devices, local(): lax.all_gather(out_new, 'fs', axis=0, tiled=True)  35.1 us
    dot_general x3, matrix products, moments(): reduced = jnp.dot(source, basis, preferred_element_type=jnp.float32)  18.3 us
  transfers between devices with their start and end apart: 6, of which 5 were waited for; matrix products, arithmetic and copies ran while one was open for 6% of the time, Pallas kernels for 0%

commit v1 on v0

v1 whole, which is shorter than its diff:
```python
import functools

import jax
import jax.numpy as jnp
from jax import lax
from jax.experimental import pallas as pl
from jax.experimental.pallas import tpu as pltpu
from jax.sharding import PartitionSpec as P

MESH = pl.DeviceIdType.MESH
ANY = pl.ANY
VMEM = pltpu.VMEM


def kernel(
    n,
    tp_n,
    chunk,
    saved_hbm,
    outcot_hbm,
    qcot_hbm,
    fcot_hbm,
    mixed_hbm,
    qb_hbm,
    fb_hbm,
    ob_hbm,
    qw,
    fw,
    ow,
    q1,
    f1,
    o1,
    q2,
    f2,
    o2,
    qup,
    fup,
    oup,
    q1n,
    f1n,
    o1n,
    q2n,
    f2n,
    o2n,
    qc,
    fc,
    oc,
    src,
    cot,
    bas,
    acc,
    part,
    rs_buf,
    dirs,
    gath,
    stage,
    sq_own,
    sq_buf,
    src_sem,
    cot_sem,
    bas_sem,
    rs_send,
    rs_recv,
    ag_send,
    ag_recv,
    w_send,
    w_recv,
    sq_send,
    sq_recv,
    out_sem,
):
    me = lax.axis_index("fs")
    tp = lax.axis_index("tp")
    weights, firsts, seconds = (qw, fw, ow), (q1, f1, o1), (q2, f2, o2)
    updates, firsts_new, seconds_new = (qup, fup, oup), (q1n, f1n, o1n), (q2n, f2n, o2n)
    copies = (qc, fc, oc)
    tokens = saved_hbm.shape[0]
    rank, cols = acc.shape
    rows = qw.shape[0]
    rp = rank // n
    n_chunks = tokens // chunk
    half = n // 2
    y = lax.rem(me, 2)
    o = me // 2
    partner = o * 2 + 1 - y

    def src_copy(s, c):
        return pltpu.make_async_copy(
            (saved_hbm, outcot_hbm)[s].at[pl.ds(c * chunk, chunk)],
            src.at[s, pl.ds(c * chunk, chunk)],
            src_sem.at[s, c],
        )

    def cot_copy(m):
        return pltpu.make_async_copy((qcot_hbm, fcot_hbm, mixed_hbm)[m], cot.at[m], cot_sem.at[m])

    def bas_copy(m):
        return pltpu.make_async_copy((qb_hbm, fb_hbm, ob_hbm)[m], bas.at[m], bas_sem.at[m])

    bas_copy(0).start()
    src_copy(0, 0).start()
    cot_copy(0).start()
    for c in range(1, n_chunks):
        src_copy(0, c).start()
    bas_copy(1).start()
    cot_copy(1).start()
    bas_copy(2).start()
    for c in range(n_chunks):
        src_copy(1, c).start()
    cot_copy(2).start()

    for m in range(3):
        gath[m, me] = weights[m][...].astype(jnp.bfloat16)

    barrier = pltpu.get_barrier_semaphore()
    for k in range(1, n):
        pl.semaphore_signal(
            barrier, inc=1, device_id={"fs": lax.rem(me + k, n)}, device_id_type=MESH
        )
    for k in range(1, tp_n):
        pl.semaphore_signal(
            barrier, inc=1, device_id={"tp": lax.rem(tp + k, tp_n)}, device_id_type=MESH
        )
    pl.semaphore_wait(barrier, n - 1 + tp_n - 1)

    def w_copy(m, block, target, send_sem):
        return pltpu.make_async_remote_copy(
            src_ref=gath.at[m, block],
            dst_ref=gath.at[m, block],
            send_sem=send_sem,
            recv_sem=w_recv.at[m, block],
            device_id={"fs": target},
            device_id_type=MESH,
        )

    def w_wait(block):
        for m in range(3):
            w_copy(m, block, partner, w_send.at[0, m, 0]).wait_recv()

    def w_round(r, act):
        below, above = o - r, o + r
        if r < half - 1:

            @pl.when(jnp.logical_and(below >= 0, o + 1 < half))
            def _():
                for m in range(3):
                    act(w_copy(m, below * 2 + y, me + 2, w_send.at[0, m, r]))

            @pl.when(jnp.logical_and(above < half, o >= 1))
            def _():
                for m in range(3):
                    act(w_copy(m, above * 2 + y, me - 2, w_send.at[1, m, r]))

        @pl.when(below >= 0)
        def _():
            for m in range(3):
                act(w_copy(m, below * 2 + y, partner, w_send.at[2, m, r]))

        if r > 0:

            @pl.when(above < half)
            def _():
                for m in range(3):
                    act(w_copy(m, above * 2 + y, partner, w_send.at[3, m, r]))

    def w_start(r):
        if r > 0:

            @pl.when(o - r >= 0)
            def _():
                w_wait((o - r) * 2 + y)

            @pl.when(o + r < half)
            def _():
                w_wait((o + r) * 2 + y)

        w_round(r, lambda copy: copy.start())

    w_start(0)

    def rs_copy(m, k):
        peer = lax.rem(me + k, n)
        return pltpu.make_async_remote_copy(
            src_ref=part.at[m, pl.ds(pl.multiple_of(peer * rp, rp), rp)],
            dst_ref=rs_buf.at[m, k - 1],
            send_sem=rs_send.at[m, k - 1],
            recv_sem=rs_recv.at[m, k - 1],
            device_id={"fs": peer},
            device_id_type=MESH,
        )

    mine = pl.ds(pl.multiple_of(me * rp, rp), rp)

    def ag_copy(m, k):
        peer = lax.rem(me + k, n)
        return pltpu.make_async_remote_copy(
            src_ref=dirs.at[m, mine],
            dst_ref=dirs.at[m, mine],
            send_sem=ag_send.at[m, k - 1],
            recv_sem=ag_recv.at[m, k - 1],
            device_id={"fs": peer},
            device_id_type=MESH,
        )

    def project(m):
        s = (0, 0, 1)[m]
        bas_copy(m).wait()
        cot_copy(m).wait()
        if m != 1:
            for c in range(n_chunks):
                src_copy(s, c).wait()

        acc[...] = jnp.zeros_like(acc)

        def body(c, carry):
            at = pl.ds(pl.multiple_of(c * chunk, chunk), chunk)
            reduced = jnp.dot(
                src[s, at, :], bas[m], preferred_element_type=jnp.float32
            ).astype(jnp.bfloat16)
            acc[...] += lax.dot_general(
                reduced,
                cot[m, at, :],
                (((0,), (0,)), ((), ())),
                preferred_element_type=jnp.float32,
            )
            return carry

        lax.fori_loop(0, n_chunks, body, 0)
        part[m] = acc[...].astype(jnp.bfloat16)
        for k in range(1, n):
            rs_copy(m, k).start()

    project(0)
    project(1)
    w_start(1)
    project(2)

    for m in range(3):
        projected = part[m, mine, :].astype(jnp.float32)
        for k in range(1, n):
            rs_copy(m, k).wait_recv()
            projected += rs_buf[m, k - 1].astype(jnp.float32)
        first_new = 0.8 * firsts[m][...] + 0.2 * projected
        second_new = 0.95 * seconds[m][...] + 0.05 * projected * projected
        firsts_new[m][...] = first_new
        seconds_new[m][...] = second_new
        direction = first_new / (jnp.sqrt(second_new) + 1e-08)
        dirs[m, mine, :] = direction.astype(jnp.bfloat16)
        for k in range(1, n):
            ag_copy(m, k).start()

    for r in range(2, half):
        w_start(r)

    sums = []
    for m in range(3):
        for k in range(1, n):
            peer = lax.rem(me + n - k, n)
            pltpu.make_async_remote_copy(
                src_ref=dirs.at[m, mine],
                dst_ref=dirs.at[m, pl.ds(pl.multiple_of(peer * rp, rp), rp)],
                send_sem=ag_send.at[m, k - 1],
                recv_sem=ag_recv.at[m, k - 1],
                device_id={"fs": peer},
                device_id_type=MESH,
            ).wait_recv()
        wide = dirs[m].astype(jnp.float32)
        sums.append(jnp.sum(wide * wide))
    line = lax.broadcasted_iota(jnp.int32, sq_own.shape, 0)
    sq_own[...] = jnp.where(line == 0, sums[0], jnp.where(line == 1, sums[1], sums[2]))

    def sq_copy(k):
        return pltpu.make_async_remote_copy(
            src_ref=sq_own,
            dst_ref=sq_buf.at[k - 1],
            send_sem=sq_send.at[k - 1],
            recv_sem=sq_recv.at[k - 1],
            device_id={"tp": lax.rem(tp + k, tp_n)},
            device_id_type=MESH,
        )

    for k in range(1, tp_n):
        sq_copy(k).start()
    total = sq_own[...]
    for k in range(1, tp_n):
        sq_copy(k).wait_recv()
        total += sq_buf[k - 1]
    scale = lax.rsqrt(total / (rank * cols * tp_n) + 1e-06)

    def out_copy(m, block):
        return pltpu.make_async_copy(
            stage.at[m, block],
            copies[m].at[pl.ds(pl.multiple_of(block * rows, rows), rows)],
            out_sem.at[m, block],
        )

    def step_of(m, block):
        at = pl.ds(pl.multiple_of(block * rows, rows), rows)
        return jnp.dot(bas[m, at, :], dirs[m], preferred_element_type=jnp.float32)

    for m in range(3):
        update = step_of(m, me) * scale[m : m + 1, :1]
        updates[m][...] = update
        stage[m, me] = (weights[m][...] - 0.05 * update).astype(jnp.bfloat16)
        out_copy(m, me).start()

    def finish(block):
        for m in range(3):
            stage[m, block] = (
                gath[m, block].astype(jnp.float32)
                - step_of(m, block) * (0.05 * scale[m : m + 1, :1])
            ).astype(jnp.bfloat16)
            out_copy(m, block).start()

    def near(i, carry):
        finish(lax.rem(o + i, half) * 2 + y)
        return carry

    def far(i, carry):
        block = lax.rem(o + i, half) * 2 + 1 - y
        w_wait(block)
        finish(block)
        return carry

    lax.fori_loop(1, half, near, 0)
    lax.fori_loop(0, half, far, 0)

    for r in range(half):
        w_round(r, lambda copy: copy.wait_send())
    for m in range(3):
        for k in range(1, n):
            rs_copy(m, k).wait_send()
            ag_copy(m, k).wait_send()
    for k in range(1, tp_n):
        sq_copy(k).wait_send()

    def drain(block, carry):
        for m in range(3):
            out_copy(m, block).wait()
        return carry

    lax.fori_loop(0, n, drain, 0)


def local(
    n,
    tp_n,
    saved_input,
    query_cotangent,
    forget_cotangent,
    mixed_output,
    out_cotangent,
    query_basis,
    forget_basis,
    out_basis,
    query_weight,
    forget_weight,
    out_weight,
    query_first,
    forget_first,
    out_first,
    query_second,
    forget_second,
    out_second,
):
    tokens, width = saved_input.shape
    rank = query_basis.shape[1]
    rows, cols = query_weight.shape
    rp = rank // n
    half = n // 2
    chunk = min(512, tokens)
    f32, bf16 = jnp.float32, jnp.bfloat16
    dma = pltpu.SemaphoreType.DMA
    shape = jax.ShapeDtypeStruct
    return pl.pallas_call(
        functools.partial(kernel, n, tp_n, chunk),
        out_shape=(shape((rows, cols), f32),) * 3
        + (shape((rp, cols), f32),) * 6
        + (shape((n * rows, cols), bf16),) * 3,
        in_specs=[pl.BlockSpec(memory_space=ANY)] * 8 + [pl.BlockSpec(memory_space=VMEM)] * 9,
        out_specs=(pl.BlockSpec(memory_space=VMEM),) * 9 + (pl.BlockSpec(memory_space=ANY),) * 3,
        scratch_shapes=[
            VMEM((2, tokens, width), bf16),
            VMEM((3, tokens, cols), bf16),
            VMEM((3, width, rank), bf16),
            VMEM((rank, cols), f32),
            VMEM((3, rank, cols), bf16),
            VMEM((3, n - 1, rp, cols), bf16),
            VMEM((3, rank, cols), bf16),
            VMEM((3, n, rows, cols), bf16),
            VMEM((3, n, rows, cols), bf16),
            VMEM((8, 128), f32),
            VMEM((tp_n - 1, 8, 128), f32),
            dma((2, tokens // chunk)),
            dma((3,)),
            dma((3,)),
            dma((3, n - 1)),
            dma((3, n - 1)),
            dma((3, n - 1)),
            dma((3, n - 1)),
            dma((4, 3, half)),
            dma((3, n)),
            dma((tp_n - 1,)),
            dma((tp_n - 1,)),
            dma((3, n)),
        ],
        compiler_params=pltpu.CompilerParams(
            collective_id=0, has_side_effects=True, vmem_limit_bytes=63 * 1024 * 1024
        ),
    )(
        saved_input,
        out_cotangent,
        query_cotangent,
        forget_cotangent,
        mixed_output,
        query_basis,
        forget_basis,
        out_basis,
        query_weight,
        forget_weight,
        out_weight,
        query_first,
        forget_first,
        out_first,
        query_second,
        forget_second,
        out_second,
    )


def solution(mesh):
    split = P("fs", "tp")
    in_specs = (
        (P("fs", None), split, split, split, P("fs", None)) + (P(),) * 3 + (split,) * 9
    )
    out_specs = (split,) * 9 + (P(None, "tp"),) * 3
    return jax.shard_map(
        functools.partial(local, mesh.shape["fs"], mesh.shape["tp"]),
        mesh=mesh,
        in_specs=in_specs,
        out_specs=out_specs,
        check_vma=False,
    )
```

time: 427 us -> 128 us (0.30)
  waiting for transfers between devices: 228 us -> 0 us
  blocking collectives: 137 us -> 0 us
  Pallas kernels: 0 us -> 111 us
  matrix products: 31.9 us -> 0 us
  between operations: 16.4 us -> 0.73 us
  local copies, waits for them, and re-layouts: 6.94 us -> 15.6 us
  other arithmetic: 6.12 us -> 0 us
    reduce_scatter x3 -> x0, waiting for transfers between devices: 142 us -> none  [moments(): lax.psum_scatter((contract_rows(reduced_high, cotangent) + contract_rows(...]
    pallas_call x0 -> x1, Pallas kernels: none -> 111 us  [local(): pl.pallas_call(functools.partial(kernel, n, tp_n, chunk), out_shape=(shap...]
    all_gather x3 -> x0, blocking collectives: 96.4 us -> none  [expand(): lax.all_gather(direction, 'fs', axis=0, tiled=True)]
    all_gather x3 -> x0, waiting for transfers between devices: 85.4 us -> none  [the longest x1 50.2 us: local(): lax.all_gather(query_new, 'fs', axis=0, tiled=True)]
    psum x1 -> x0, blocking collectives: 40.4 us -> none  [local(): totals = lax.psum((query_sq, forget_sq, out_sq), ('fs', 'tp'))]
    dot_general x12 -> x0, matrix products: 31.9 us -> none  [the longest x3 18.3 us: moments(): reduced = jnp.dot(source, basis, preferred_element_type=jnp.float32)]
    unnamed x33 -> x30, local copies, waits for them, and re-layouts: 6.94 us -> 15.6 us
    reduce_sum x3 -> x0, other arithmetic: 6.12 us -> none  [moments(): jnp.sum(direction * direction)]
  transfers between devices with their start and end apart: 6 -> 0, of which waited for: 5 -> 0; matrix products, arithmetic and copies ran while one was open for 6% -> 0% of each run, Pallas kernels for 0% -> 0%
where the time goes in v1:
time: 128 us; the launch traced here: 127 us
  Pallas kernels  111 us (87%)
  local copies, waits for them, and re-layouts  15.6 us (12%)
    pallas_call x1, Pallas kernels, local(): pl.pallas_call(functools.partial(kernel, n, tp_n, chunk), out_shape=(shap...  111 us
    unnamed x30, local copies, waits for them, and re-layouts  15.6 us

profile of v1, /device:TPU:0, one launch (start us, length us, event | category | flops | bytes accessed | tf_op | source)
XLA Modules:
  0.0 127.2 jit_solution(10848466523650745907)
XLA Ops:
  0.7 110.9 %shard_map.256 = (f32[256,512]{1,0:T(8,128)}, f32[256,512]{1,0:T(8,128)}, f32[256,512]{1,0:T(8,128)}, f32[32,512]{1,0:T(8,128)}, f32[32,512]{1,0:T(8,128)}, /*in...) custom-call(bf16[2048,2048]{1,0:T(8,128)(2,1)} %saved_hbm.1, ...), custom_call_target="tpu_custom_call" | custom-call | tf_op jit(solution)/shard_map/pallas_call | solution.py:375
  111.5 0.0 copy-start.8
  111.5 0.0 copy-start.7
  111.5 0.0 copy-start.6
  111.5 0.0 copy-start.5
  111.6 0.0 copy-start.4
  111.6 0.0 copy-start.3
  111.6 0.0 copy-start.2
  111.6 2.0 %copy.41 = f32[256,512]{1,0:T(8,128)} copy(f32[256,512]{1,0:T(8,128)} %get-tuple-element.24) | data formatting | bytes 1048576
  113.6 1.9 %copy.42 = f32[256,512]{1,0:T(8,128)} copy(f32[256,512]{1,0:T(8,128)} %get-tuple-element.25) | data formatting | bytes 1048576
  115.5 1.9 %copy.43 = f32[256,512]{1,0:T(8,128)} copy(f32[256,512]{1,0:T(8,128)} %get-tuple-element.26) | data formatting | bytes 1048576
  117.3 0.0 copy-done.8
  117.3 0.6 copy.44
  118.0 0.6 copy.45
  118.6 0.0 copy-done.6
  118.6 0.6 copy.46
  119.2 0.6 copy.47
  119.9 0.6 copy.48
  120.5 0.6 copy.49
  121.1 1.3 %copy.50 = bf16[2048,512]{1,0:T(8,128)(2,1)} copy(bf16[2048,512]{1,0:T(8,128)(2,1)S(1)} %copy-done.2) | data formatting | bytes 4194304
  122.5 1.0 copy-done.1
  123.5 1.3 %copy.51 = bf16[2048,512]{1,0:T(8,128)(2,1)} copy(bf16[2048,512]{1,0:T(8,128)(2,1)S(1)} %copy-done.1) | data formatting | bytes 4194304
  124.8 1.0 copy-done
  125.8 1.3 %copy.52 = bf16[2048,512]{1,0:T(8,128)(2,1)} copy(bf16[2048,512]{1,0:T(8,128)(2,1)S(1)} %copy-done) | data formatting | bytes 4194304
  (7 shorter events, 0.0 us)
Async XLA Ops:
  111.5 5.8 %copy-start.8 = (f32[32,512]{1,0:T(8,128)S(1)}, f32[32,512]{1,0:T(8,128)}, u32[]{:S(2)}) copy-start(f32[32,512]{1,0:T(8,128)} %get-tuple-element.27) | copy-start | bytes 196612
  111.5 6.5 %copy-start.7 = (f32[32,512]{1,0:T(8,128)S(1)}, f32[32,512]{1,0:T(8,128)}, u32[]{:S(2)}) copy-start(f32[32,512]{1,0:T(8,128)} %get-tuple-element.28) | copy-start | bytes 196612
  111.5 7.1 %copy-start.6 = (f32[32,512]{1,0:T(8,128)S(1)}, f32[32,512]{1,0:T(8,128)}, u32[]{:S(2)}) copy-start(f32[32,512]{1,0:T(8,128)} %get-tuple-element.29) | copy-start | bytes 196612
  111.5 7.7 %copy-start.5 = (f32[32,512]{1,0:T(8,128)S(1)}, f32[32,512]{1,0:T(8,128)}, u32[]{:S(2)}) copy-start(f32[32,512]{1,0:T(8,128)} %get-tuple-element.30) | copy-start | bytes 196612
  111.6 8.3 %copy-start.4 = (f32[32,512]{1,0:T(8,128)S(1)}, f32[32,512]{1,0:T(8,128)}, u32[]{:S(2)}) copy-start(f32[32,512]{1,0:T(8,128)} %get-tuple-element.31) | copy-start | bytes 196612
  111.6 8.9 %copy-start.3 = (f32[32,512]{1,0:T(8,128)S(1)}, f32[32,512]{1,0:T(8,128)}, u32[]{:S(2)}) copy-start(f32[32,512]{1,0:T(8,128)} %get-tuple-element.32) | copy-start | bytes 196612
  111.6 9.6 %copy-start.2 = (bf16[2048,512]{1,0:T(8,128)(2,1)S(1)}, bf16[2048,512]{1,0:T(8,128)(2,1)}, u32[]{:S(2)}) copy-start(bf16[2048,512]{1,0:T(8,128)(2,1)} %get-tuple-element.33) | copy-start | bytes 6291460
  121.1 2.3 %copy-start.1 = (bf16[2048,512]{1,0:T(8,128)(2,1)S(1)}, bf16[2048,512]{1,0:T(8,128)(2,1)}, u32[]{:S(2)}) copy-start(bf16[2048,512]{1,0:T(8,128)(2,1)} %get-tuple-element.34) | copy-start | bytes 6291460
  123.5 2.3 %copy-start = (bf16[2048,512]{1,0:T(8,128)(2,1)S(1)}, bf16[2048,512]{1,0:T(8,128)(2,1)}, u32[]{:S(2)}) copy-start(bf16[2048,512]{1,0:T(8,128)(2,1)} %get-tuple-element.35) | copy-start | bytes 6291460

commit v2 on v1

--- a/solution.py
+++ b/solution.py
@@ -97,6 +97,16 @@
     def bas_copy(m):
         return pltpu.make_async_copy((qb_hbm, fb_hbm, ob_hbm)[m], bas.at[m], bas_sem.at[m])
 
+    barrier = pltpu.get_barrier_semaphore()
+    for k in range(1, n):
+        pl.semaphore_signal(
+            barrier, inc=1, device_id={"fs": lax.rem(me + k, n)}, device_id_type=MESH
+        )
+    for k in range(1, tp_n):
+        pl.semaphore_signal(
+            barrier, inc=1, device_id={"tp": lax.rem(tp + k, tp_n)}, device_id_type=MESH
+        )
+
     bas_copy(0).start()
     src_copy(0, 0).start()
     cot_copy(0).start()
@@ -112,15 +122,6 @@
     for m in range(3):
         gath[m, me] = weights[m][...].astype(jnp.bfloat16)
 
-    barrier = pltpu.get_barrier_semaphore()
-    for k in range(1, n):
-        pl.semaphore_signal(
-            barrier, inc=1, device_id={"fs": lax.rem(me + k, n)}, device_id_type=MESH
-        )
-    for k in range(1, tp_n):
-        pl.semaphore_signal(
-            barrier, inc=1, device_id={"tp": lax.rem(tp + k, tp_n)}, device_id_type=MESH
-        )
     pl.semaphore_wait(barrier, n - 1 + tp_n - 1)
 
     def w_copy(m, block, target, send_sem):
@@ -133,48 +134,43 @@
             device_id_type=MESH,
         )
 
-    def w_wait(block):
+    def w_arrived(m, block):
+        w_copy(m, block, partner, w_send.at[0, m, 0]).wait_recv()
+
+    def w_round(r, act, wait, z=True, side=True):
+        below, above = o - r, o + r
         for m in range(3):
-            w_copy(m, block, partner, w_send.at[0, m, 0]).wait_recv()
-
-    def w_round(r, act):
-        below, above = o - r, o + r
-        if r < half - 1:
-
-            @pl.when(jnp.logical_and(below >= 0, o + 1 < half))
+
+            @pl.when(below >= 0)
             def _():
-                for m in range(3):
-                    act(w_copy(m, below * 2 + y, me + 2, w_send.at[0, m, r]))
-
-            @pl.when(jnp.logical_and(above < half, o >= 1))
-            def _():
-                for m in range(3):
-                    act(w_copy(m, above * 2 + y, me - 2, w_send.at[1, m, r]))
-
-        @pl.when(below >= 0)
-        def _():
-            for m in range(3):
-                act(w_copy(m, below * 2 + y, partner, w_send.at[2, m, r]))
-
-        if r > 0:
+                block = below * 2 + y
+                if wait and r > 0:
+                    w_arrived(m, block)
+                if z and r < half - 1:
+
+                    @pl.when(o + 1 < half)
+                    def _():
+                        act(w_copy(m, block, me + 2, w_send.at[0, m, r]))
+
+                if side:
+                    act(w_copy(m, block, partner, w_send.at[2, m, r]))
 
             @pl.when(above < half)
             def _():
-                for m in range(3):
-                    act(w_copy(m, above * 2 + y, partner, w_send.at[3, m, r]))
-
-    def w_start(r):
-        if r > 0:
-
-            @pl.when(o - r >= 0)
-            def _():
-                w_wait((o - r) * 2 + y)
-
-            @pl.when(o + r < half)
-            def _():
-                w_wait((o + r) * 2 + y)
-
-        w_round(r, lambda copy: copy.start())
+                block = above * 2 + y
+                if wait and r > 0:
+                    w_arrived(m, block)
+                if z and r < half - 1:
+
+                    @pl.when(o >= 1)
+                    def _():
+                        act(w_copy(m, block, me - 2, w_send.at[1, m, r]))
+
+                if side and r > 0:
+                    act(w_copy(m, block, partner, w_send.at[3, m, r]))
+
+    def w_start(r, z=True, side=True):
+        w_round(r, lambda copy: copy.start(), z, z, side)
 
     w_start(0)
 
@@ -191,16 +187,27 @@
 
     mine = pl.ds(pl.multiple_of(me * rp, rp), rp)
 
-    def ag_copy(m, k):
-        peer = lax.rem(me + k, n)
+    def ag_copy(m, block, target, slot):
+        at = pl.ds(pl.multiple_of(block * rp, rp), rp)
         return pltpu.make_async_remote_copy(
-            src_ref=dirs.at[m, mine],
-            dst_ref=dirs.at[m, mine],
-            send_sem=ag_send.at[m, k - 1],
-            recv_sem=ag_recv.at[m, k - 1],
-            device_id={"fs": peer},
+            src_ref=dirs.at[m, at],
+            dst_ref=dirs.at[m, at],
+            send_sem=ag_send.at[m, slot],
+            recv_sem=ag_recv.at[m, block],
+            device_id={"fs": target},
             device_id_type=MESH,
         )
+
+    def ag_own(m):
+        return [ag_copy(m, me, partner, 0)] + [
+            ag_copy(m, me, lax.rem(o + d, half) * 2 + y, d) for d in range(1, half)
+        ]
+
+    def ag_forward(m):
+        return [
+            ag_copy(m, partner, lax.rem(o + d, half) * 2 + y, half - 1 + d)
+            for d in range(1, half)
+        ]
 
     def project(m):
         s = (0, 0, 1)[m]
@@ -232,8 +239,8 @@
 
     project(0)
     project(1)
+    project(2)
     w_start(1)
-    project(2)
 
     for m in range(3):
         projected = part[m, mine, :].astype(jnp.float32)
@@ -246,24 +253,23 @@
         seconds_new[m][...] = second_new
         direction = first_new / (jnp.sqrt(second_new) + 1e-08)
         dirs[m, mine, :] = direction.astype(jnp.bfloat16)
-        for k in range(1, n):
-            ag_copy(m, k).start()
+        for copy in ag_own(m):
+            copy.start()
+
+    for m in range(3):
+        ag_copy(m, partner, partner, 0).wait_recv()
+        for copy in ag_forward(m):
+            copy.start()
 
     for r in range(2, half):
         w_start(r)
 
     sums = []
     for m in range(3):
-        for k in range(1, n):
-            peer = lax.rem(me + n - k, n)
-            pltpu.make_async_remote_copy(
-                src_ref=dirs.at[m, mine],
-                dst_ref=dirs.at[m, pl.ds(pl.multiple_of(peer * rp, rp), rp)],
-                send_sem=ag_send.at[m, k - 1],
-                recv_sem=ag_recv.at[m, k - 1],
-                device_id={"fs": peer},
-                device_id_type=MESH,
-            ).wait_recv()
+        for d in range(1, half):
+            for column in range(2):
+                block = lax.rem(o + d, half) * 2 + column
+                ag_copy(m, block, partner, 0).wait_recv()
         wide = dirs[m].astype(jnp.float32)
         sums.append(jnp.sum(wide * wide))
     line = lax.broadcasted_iota(jnp.int32, sq_own.shape, 0)
@@ -304,33 +310,39 @@
         stage[m, me] = (weights[m][...] - 0.05 * update).astype(jnp.bfloat16)
         out_copy(m, me).start()
 
-    def finish(block):
+    def finish(block, wait):
         for m in range(3):
+            if wait:
+                w_arrived(m, block)
             stage[m, block] = (
                 gath[m, block].astype(jnp.float32)
                 - step_of(m, block) * (0.05 * scale[m : m + 1, :1])
             ).astype(jnp.bfloat16)
             out_copy(m, block).start()
 
-    def near(i, carry):
-        finish(lax.rem(o + i, half) * 2 + y)
-        return carry
-
-    def far(i, carry):
-        block = lax.rem(o + i, half) * 2 + 1 - y
-        w_wait(block)
-        finish(block)
-        return carry
-
-    lax.fori_loop(1, half, near, 0)
-    lax.fori_loop(0, half, far, 0)
+    def finish_at(distance, column, wait):
+        @pl.when(o - distance >= 0)
+        def _():
+            finish((o - distance) * 2 + column, wait)
+
+        if distance > 0:
+
+            @pl.when(o + distance < half)
+            def _():
+                finish((o + distance) * 2 + column, wait)
+
+    finish_at(0, 1 - y, True)
+    for d in range(1, half):
+        finish_at(d, y, False)
+        finish_at(d, 1 - y, True)
 
     for r in range(half):
-        w_round(r, lambda copy: copy.wait_send())
+        w_round(r, lambda copy: copy.wait_send(), False)
     for m in range(3):
         for k in range(1, n):
             rs_copy(m, k).wait_send()
-            ag_copy(m, k).wait_send()
+        for copy in ag_own(m) + ag_forward(m):
+            copy.wait_send()
     for k in range(1, tp_n):
         sq_copy(k).wait_send()
 
@@ -340,6 +352,48 @@
         return carry
 
     lax.fori_loop(0, n, drain, 0)
+
+
+def deliver(count, *refs):
+    sources, targets, slots = refs[:count], refs[count : 2 * count], refs[2 * count : 3 * count]
+    in_sem, out_sem = refs[3 * count :]
+
+    def pieces(act_in, act_out):
+        for i in range(count):
+            rows = sources[i].shape[0]
+            step = max(rows // 4, rows if rows <= 256 else 0)
+            for p in range(rows // step):
+                at = pl.ds(p * step, step)
+                if act_in:
+                    act_in(
+                        pltpu.make_async_copy(
+                            sources[i].at[at], slots[i].at[at], in_sem.at[i, p]
+                        )
+                    )
+                if act_out:
+                    act_out(
+                        pltpu.make_async_copy(
+                            slots[i].at[at], targets[i].at[at], out_sem.at[i, p]
+                        )
+                    )
+
+    pieces(lambda copy: copy.start(), None)
+    pieces(lambda copy: copy.wait(), lambda copy: copy.start())
+    pieces(None, lambda copy: copy.wait())
+
+
+def delivered(arrays):
+    count = len(arrays)
+    dma = pltpu.SemaphoreType.DMA
+    return pl.pallas_call(
+        functools.partial(deliver, count),
+        out_shape=tuple(jax.ShapeDtypeStruct(a.shape, a.dtype) for a in arrays),
+        in_specs=[pl.BlockSpec(memory_space=ANY)] * count,
+        out_specs=(pl.BlockSpec(memory_space=ANY),) * count,
+        scratch_shapes=[VMEM(a.shape, a.dtype) for a in arrays]
+        + [dma((count, 4)), dma((count, 4))],
+        compiler_params=pltpu.CompilerParams(vmem_limit_bytes=63 * 1024 * 1024),
+    )(*arrays)
 
 
 def local(
@@ -372,7 +426,7 @@
     f32, bf16 = jnp.float32, jnp.bfloat16
     dma = pltpu.SemaphoreType.DMA
     shape = jax.ShapeDtypeStruct
-    return pl.pallas_call(
+    results = pl.pallas_call(
         functools.partial(kernel, n, tp_n, chunk),
         out_shape=(shape((rows, cols), f32),) * 3
         + (shape((rp, cols), f32),) * 6
@@ -397,7 +451,7 @@
             dma((3, n - 1)),
             dma((3, n - 1)),
             dma((3, n - 1)),
-            dma((3, n - 1)),
+            dma((3, n)),
             dma((4, 3, half)),
             dma((3, n)),
             dma((tp_n - 1,)),
@@ -426,6 +480,7 @@
         forget_second,
         out_second,
     )
+    return delivered(results)
 
 
 def solution(mesh):

time: 128 us -> 111 us (0.87)
  local copies, waits for them, and re-layouts: 15.6 us -> 0 us
    unnamed x30 -> x0, local copies, waits for them, and re-layouts: 15.6 us -> none
    pallas_call x1, Pallas kernels: 111 us -> 103 us  [local(): pl.pallas_call(functools.partial(kernel, n, tp_n, chunk), out_shape=(shap...]
    pallas_call x0 -> x1, Pallas kernels: none -> 7.06 us  [delivered(): pl.pallas_call(functools.partial(deliver, count), out_shape=tuple((jax.Sh...]
where the time goes in v2:
time: 111 us
  Pallas kernels  110 us (99%)
    pallas_call x1, Pallas kernels, local(): pl.pallas_call(functools.partial(kernel, n, tp_n, chunk), out_shape=(shap...  103 us
    pallas_call x1, Pallas kernels, delivered(): pl.pallas_call(functools.partial(deliver, count), out_shape=tuple((jax.Sh...  7.06 us

profile of v2, /device:TPU:0, one launch (start us, length us, event | category | flops | bytes accessed | tf_op | source)
XLA Modules:
  0.0 110.8 jit_solution(4455409721011373510)
XLA Ops:
  0.7 103.0 %shard_map.256 = (f32[256,512]{1,0:T(8,128)}, f32[256,512]{1,0:T(8,128)}, f32[256,512]{1,0:T(8,128)}, f32[32,512]{1,0:T(8,128)}, f32[32,512]{1,0:T(8,128)}, /*in...) custom-call(bf16[2048,2048]{1,0:T(8,128)(2,1)} %saved_hbm.1, ...), custom_call_target="tpu_custom_call" | custom-call | tf_op jit(solution)/shard_map/pallas_call | solution.py:429
  103.7 7.1 %shard_map.257 = (f32[256,512]{1,0:T(8,128)}, f32[256,512]{1,0:T(8,128)}, f32[256,512]{1,0:T(8,128)}, f32[32,512]{1,0:T(8,128)}, f32[32,512]{1,0:T(8,128)}, /*in...) custom-call(f32[256,512]{1,0:T(8,128)} %get-tuple-element.24.refs_0_, ...), custom_call_target="tpu_custom_call" | custom-call | tf_op jit(solution)/shard_map/pallas_call | solution.py:388
